TPU v7x, 32 devices: a whole 2x2x4 slice. The times are simulated.
32 devices in a mesh: rep: 2 (over x), fs: 8 (over z, y), tp: 2 (over core).
Axes of the slice: x: 2, y: 2, z: 4, core: 2. Of those that a mesh axis runs over, the one named last changes fastest.
Arguments:
- tokens_in: bfloat16 [4096, 2048], P(('rep', 'fs', 'tp')), may hold values from -6 to 6
- norm_gains: float32 [3, 2048], replicated, may hold values from 0.1 to 1.9
- gate_w: float32 [2048, 3072], P('fs', 'tp'), may hold values from -0.125 to 0.125
- gate_scale: float32 [3072], P('tp'), may hold values from 0.5 to 2
- up_w: float32 [2048, 3072], P('fs', 'tp'), may hold values from -0.125 to 0.125
- up_scale: float32 [3072], P('tp'), may hold values from 0.5 to 2
- down_w: float32 [3072, 2048], P('tp', 'fs'), may hold values from -0.109375 to 0.109375
- down_scale: float32 [2048], P('fs'), may hold values from 0.5 to 2
- query_w: float32 [2048, 2048], P('fs', 'tp'), may hold values from -0.125 to 0.125
- query_scale: float32 [2048], P('tp'), may hold values from 0.5 to 2
- key_w: float32 [2048, 2048], P('fs', 'tp'), may hold values from -0.125 to 0.125
- key_scale: float32 [2048], P('tp'), may hold values from 0.5 to 2
- value_w: float32 [2048, 2048], P('fs', 'tp'), may hold values from -0.125 to 0.125
- value_scale: float32 [2048], P('tp'), may hold values from 0.5 to 2
- out_w: float32 [2048, 2048], P('tp', 'fs'), may hold values from -0.125 to 0.125
- out_scale: float32 [2048], P('fs'), may hold values from 0.5 to 2
- head_gain: float32 [256], replicated, may hold values from 0.1 to 1.9
- decay_rate: float32 [8], P('tp'), may hold values from 0 to 1, as said below
Outputs:
- tokens_out: bfloat16 [4096, 2048], P(('rep', 'fs', 'tp'))
Inputs may be any that keep to these rules, and one draw needn't show every extreme that they name: `decay_rate`: each head's decay per position, positive.
All inputs are finite; a program needn't handle non-finite values.
Results may differ from a plain program's by a relative error of at most 0.02.
Values may be sent and summed in bfloat16 or wider, within the bound.
A program may use at most 128 MiB of HBM per device.

v0:
```python
import math
import jax
import jax.numpy as jnp
from jax import lax
from jax.sharding import PartitionSpec as P

DK = 256
DV = 256
BLOCK = 64
EPSILON = 1e-05


def rms_scale(stream, gain):
    return stream * lax.rsqrt(jnp.mean(stream * stream, axis=-1, keepdims=True) + EPSILON) * gain


def retain(query, key_rows, value, decay_rate, head_gain):
    seq_len = query.shape[0]
    blocks = seq_len // BLOCK
    local_heads = decay_rate.shape[0]
    q_heads = query.reshape(blocks, BLOCK, local_heads, DK).transpose(0, 2, 1, 3)
    k_heads = key_rows.reshape(blocks, BLOCK, local_heads, DK).transpose(0, 2, 1, 3)
    v_heads = value.reshape(blocks, BLOCK, local_heads, DV).transpose(0, 2, 1, 3)
    offsets = jnp.arange(BLOCK, dtype=jnp.float32)
    inner_decay = jnp.exp(-decay_rate[:, None, None] * jnp.abs(offsets[:, None] - offsets[None, :]))
    query_decay = jnp.exp(-decay_rate[:, None] * offsets[None, :])[..., None]
    key_decay = jnp.exp(-decay_rate[:, None] * (BLOCK - offsets)[None, :])[..., None]
    block_decay = jnp.exp(-decay_rate * BLOCK)[:, None, None]

    def advance(state, inputs):
        q_blk, k_blk, v_blk = inputs
        scores = (
            jnp.einsum("hid,hjd->hij", q_blk, k_blk, preferred_element_type=jnp.float32)
            * inner_decay
        )
        scores = scores.astype(jnp.bfloat16)
        within = jnp.einsum("hij,hje->hie", scores, v_blk, preferred_element_type=jnp.float32)
        carried = jnp.einsum(
            "hid,hde->hie",
            q_blk.astype(jnp.float32) * query_decay,
            state,
            precision=lax.Precision.HIGHEST,
        )
        k_weighted = k_blk.astype(jnp.float32) * key_decay
        state = state * block_decay + jnp.einsum(
            "hjd,hje->hde", k_weighted, v_blk.astype(jnp.float32), precision=lax.Precision.HIGHEST
        )
        return (state, within + carried)

    initial = jnp.zeros((local_heads, DK, DV), jnp.float32)
    _, retained = lax.scan(advance, initial, (q_heads, k_heads, v_heads))
    retained = retained.transpose(0, 2, 1, 3).reshape(seq_len, local_heads, DV)
    centred = retained - jnp.mean(retained, axis=-1, keepdims=True)
    normed = (
        centred
        * lax.rsqrt(jnp.mean(centred * centred, axis=-1, keepdims=True) + EPSILON)
        * head_gain
    )
    return normed.reshape(seq_len, local_heads * DV).astype(jnp.bfloat16)


def on_device(
    tokens_in,
    norm_gains,
    gate_w,
    gate_scale,
    up_w,
    up_scale,
    down_w,
    down_scale,
    query_w,
    query_scale,
    key_w,
    key_scale,
    value_w,
    value_scale,
    out_w,
    out_scale,
    head_gain,
    decay_rate,
):
    down_cols, out_cols = (
        lax.all_gather(down_scale, "fs", axis=0, tiled=True),
        lax.all_gather(out_scale, "fs", axis=0, tiled=True),
    )
    gate_b = gate_w.astype(jnp.bfloat16)
    up_b = up_w.astype(jnp.bfloat16)
    down_b = down_w.astype(jnp.bfloat16)
    query_b = query_w.astype(jnp.bfloat16)
    key_b = key_w.astype(jnp.bfloat16)
    value_b = value_w.astype(jnp.bfloat16)
    out_b = out_w.astype(jnp.bfloat16)

    def gather_rows(normed):
        return lax.all_gather(normed, "tp", axis=0, tiled=True)

    def return_rows(hidden, weight, scale):
        return lax.psum_scatter(
            (jnp.dot(hidden, weight, preferred_element_type=jnp.float32) * scale).astype(
                jnp.bfloat16
            ),
            "tp",
            scatter_dimension=0,
            tiled=True,
        ).astype(jnp.float32)

    def feed_forward(stream, gain, weights):
        gate_full, up_full, down_full = weights
        gathered = gather_rows(rms_scale(stream, gain).astype(jnp.bfloat16))
        gate_value = jnp.dot(gathered, gate_full, preferred_element_type=jnp.float32) * gate_scale
        up_value = jnp.dot(gathered, up_full, preferred_element_type=jnp.float32) * up_scale
        hidden = (jax.nn.silu(gate_value) * up_value).astype(jnp.bfloat16)
        return return_rows(hidden, down_full, down_cols)

    stream = tokens_in.astype(jnp.float32)
    held = (
        lax.all_gather(gate_b, "fs", axis=0, tiled=True),
        lax.all_gather(up_b, "fs", axis=0, tiled=True),
        lax.all_gather(down_b, "fs", axis=1, tiled=True),
    )
    stream = stream + 0.5 * feed_forward(stream, norm_gains[0], held)
    gathered = gather_rows(rms_scale(stream, norm_gains[1]).astype(jnp.bfloat16))
    segments = (
        lax.all_gather(query_b, "fs", axis=0, tiled=True),
        lax.all_gather(key_b, "fs", axis=0, tiled=True),
        lax.all_gather(value_b, "fs", axis=0, tiled=True),
    )
    query_raw, key_raw, value_raw = tuple(
        (jnp.dot(gathered, segment_w, preferred_element_type=jnp.float32) for segment_w in segments)
    )
    out_full = lax.all_gather(out_b, "fs", axis=1, tiled=True)
    query = (query_raw * query_scale).astype(jnp.bfloat16)
    key_rows = (key_raw * key_scale / math.sqrt(DK)).astype(jnp.bfloat16)
    value = (value_raw * value_scale).astype(jnp.bfloat16)
    mixed = retain(query, key_rows, value, decay_rate, head_gain)
    stream = stream + return_rows(mixed, out_full, out_cols)
    stream = stream + 0.5 * feed_forward(stream, norm_gains[2], held)
    return stream.astype(jnp.bfloat16)


def solution(mesh):
    placed = (
        P(("rep", "fs", "tp"), None),
        P(),
        P("fs", "tp"),
        P("tp"),
        P("fs", "tp"),
        P("tp"),
        P("tp", "fs"),
        P("fs"),
        P("fs", "tp"),
        P("tp"),
        P("fs", "tp"),
        P("tp"),
        P("fs", "tp"),
        P("tp"),
        P("tp", "fs"),
        P("fs"),
        P(),
        P("tp"),
    )
    return jax.shard_map(
        on_device,
        mesh=mesh,
        in_specs=placed,
        out_specs=P(("rep", "fs", "tp"), None),
        check_vma=False,
    )
```

profile of v0, /device:TPU:0, one launch (start us, length us, event | category | flops | bytes accessed | tf_op | source)
XLA Modules:
  0.0 710.0 jit_solution(120403836943691048)
XLA Ops:
  11.9 2.5 convert_element_type.85
  15.5 22.3 %all-gather = f32[8,1,256]{2,1,0:T(1,128)S(1)} all-gather(f32[1,1,256]{2,1,0:T(1,128)S(1)} %bitcast.114), channel_id=1, replica_groups=mesh['rep'=2,'fs'=8,'tp'=2] {'fs'}, dimensions={0}, use_global_device_ids=true | all-gather | bytes 9216 | tf_op jit(solution)/shard_map/all_gather | solution.py:83
  37.9 86.9 %all-gather.15.cloned.1.call-done = bf16[2048,1536]{1,0:T(8,128)(2,1)} async-done(((bf16[256,1536]{1,0:T(8,128)(2,1)}), bf16[2048,1536]{1,0:T(8,128)(2,1)}) %all-gather.15.cloned.1.call-update) | async-done | bytes 6291472 | tf_op jit(solution)/shard_map/all_gather | solution.py:117
  124.8 6.1 convolution_multiply_fusion.4
  130.8 93.0 %all-gather.17.cloned.1.call-done = bf16[2048,1536]{1,0:T(8,128)(2,1)} async-done(((bf16[256,1536]{1,0:T(8,128)(2,1)}), bf16[2048,1536]{1,0:T(8,128)(2,1)}) %all-gather.17.cloned.1.call-update) | async-done | bytes 6291472 | tf_op jit(solution)/shard_map/all_gather | solution.py:118
  223.9 99.6 %all-gather.19.cloned.1.call-done = bf16[1536,2048]{1,0:T(8,128)(2,1)} async-done(((bf16[1536,256]{1,0:T(8,128)(2,1)}), bf16[1536,2048]{1,0:T(8,128)(2,1)}) %all-gather.19.cloned.1.call-update) | async-done | bytes 6291472 | tf_op jit(solution)/shard_map/all_gather | solution.py:119
  323.5 9.6 %fusion.46 = bf16[256,2048]{1,0:T(8,128)(2,1)} fusion(bf16[1536,2048]{1,0:T(8,128)(2,1)} %all-gather.19.cloned.1.call-done, f32[2048]{0:T(1024)S(1)} %bitcast.112, bf16[256,2048]{1,0:T(8,128)(2,1)S(1)} %copy-done.13, bf16[2048,1536]{1,0:T(8,128)(2,1)} %all-gather.17.cloned.1.call-done, f32[256,1536]{1,0:T(8,128)} %convolution_multiply_fusion.4, ...), kind=kOutput, calls=%fused_computation.50 | convolution fusion | flops 3225026560 | bytes 16267264 | tf_op jit(solution)/shard_map/dot_general | solution.py:99
  334.1 5.7 reduce-scatter.4.cloned.1.call-done
  346.7 21.5 %all-gather.1 = f32[8,1,256]{2,1,0:T(1,128)S(1)} all-gather(f32[1,1,256]{2,1,0:T(1,128)S(1)} %bitcast.115), channel_id=1, replica_groups=mesh['rep'=2,'fs'=8,'tp'=2] {'fs'}, dimensions={0}, use_global_device_ids=true | all-gather | bytes 9216 | tf_op jit(solution)/shard_map/all_gather | solution.py:84
  368.2 47.7 %all-gather.25.cloned.1.call-done = bf16[2048,1024]{1,0:T(8,128)(2,1)} async-done(((bf16[256,1024]{1,0:T(8,128)(2,1)}), bf16[2048,1024]{1,0:T(8,128)(2,1)}) %all-gather.25.cloned.1.call-update) | async-done | bytes 4194320 | tf_op jit(solution)/shard_map/all_gather | solution.py:126
  415.9 9.1 %all-gather.21.cloned.1.call-done = bf16[256,2048]{1,0:T(8,128)(2,1)} async-done(((bf16[128,2048]{1,0:T(8,128)(2,1)}), bf16[256,2048]{1,0:T(8,128)(2,1)}) %all-gather.21.cloned.1.call-update) | async-done | bytes 1048592 | tf_op jit(solution)/shard_map/all_gather | solution.py:95
  425.1 3.8 fusion.53
  430.0 71.2 %all-gather.27.cloned.1.call-done = bf16[2048,1024]{1,0:T(8,128)(2,1)} async-done(((bf16[256,1024]{1,0:T(8,128)(2,1)}), bf16[2048,1024]{1,0:T(8,128)(2,1)}) %all-gather.27.cloned.1.call-update) | async-done | bytes 4194320 | tf_op jit(solution)/shard_map/all_gather | solution.py:124
  501.2 3.8 fusion.54
  506.1 68.6 %all-gather.23.cloned.1.call-done = bf16[2048,1024]{1,0:T(8,128)(2,1)} async-done(((bf16[256,1024]{1,0:T(8,128)(2,1)}), bf16[2048,1024]{1,0:T(8,128)(2,1)}) %all-gather.23.cloned.1.call-update) | async-done | bytes 4194320 | tf_op jit(solution)/shard_map/all_gather | solution.py:125
  574.7 3.8 fusion.52
  583.1 19.4 %while.15 = (s32[]{:T(128)}, f32[4,256,256]{2,1,0:T(8,128)S(1)}, f32[4,4,64,256]{3,2,1,0:T(8,128)S(1)}, f32[4,1,1]{0,2,1:T(1,128)S(1)}, bf16[4,4,64,256]{3,2,1,0...) while((s32[]{:T(128)}, f32[4,256,256]{2,1,0:T(8,128)S(1)}, ...), condition=%wide.region_4.5_spmd.clone.clone.clone, body=%wide.region_3.4_spmd.clone.clone.clone.sunk | while | flops 420856320 | bytes 4761488 | solution.py:51
  607.4 42.4 %all-gather.29.cloned.1.call-done = bf16[1024,2048]{1,0:T(8,128)(2,1)} async-done(((bf16[1024,256]{1,0:T(8,128)(2,1)}), bf16[1024,2048]{1,0:T(8,128)(2,1)}) %all-gather.29.cloned.1.call-update) | async-done | bytes 4194320 | tf_op jit(solution)/shard_map/all_gather | solution.py:131
  649.8 5.2 fusion.48
  655.0 6.7 reduce-scatter.6.cloned.1.call-done
  665.6 10.1 %all-gather.31.cloned.1.call-done = bf16[256,2048]{1,0:T(8,128)(2,1)} async-done(((bf16[128,2048]{1,0:T(8,128)(2,1)}), bf16[256,2048]{1,0:T(8,128)(2,1)}) %all-gather.31.cloned.1.call-update) | async-done | bytes 1048592 | tf_op jit(solution)/shard_map/all_gather | solution.py:95
  675.8 6.1 convolution_multiply_fusion.2
  681.9 9.6 %fusion.47 = bf16[256,2048]{1,0:T(8,128)(2,1)} fusion(bf16[1536,2048]{1,0:T(8,128)(2,1)} %all-gather.19.cloned.1.call-done, f32[2048]{0:T(1024)S(1)} %bitcast.113, bf16[256,2048]{1,0:T(8,128)(2,1)S(1)} %copy-done.14, bf16[2048,1536]{1,0:T(8,128)(2,1)} %all-gather.17.cloned.1.call-done, f32[256,1536]{1,0:T(8,128)} %convolution_multiply_fusion.2, ...), kind=kOutput, calls=%fused_computation.51 | convolution fusion | flops 3225026560 | bytes 16267264 | tf_op jit(solution)/shard_map/dot_general | solution.py:99
  691.5 9.7 %reduce-scatter.8.cloned.1.call-done = bf16[128,2048]{1,0:T(8,128)(2,1)} async-done(((bf16[256,2048]{1,0:T(8,128)(2,1)}), bf16[128,2048]{1,0:T(8,128)(2,1)}) %reduce-scatter.8.cloned.1.call-update) | async-done | bytes 524304 | tf_op jit(solution)/shard_map/reduce_scatter | solution.py:98
  (126 shorter events, 51.5 us)
Async XLA Ops:
  6.5 340.1 %copy-start = (f32[256]{0:T(256)S(1)}, f32[256]{0:T(256)}, u32[]{:S(2)}) copy-start(f32[256]{0:T(256)} %param.36) | copy-start | bytes 3076
  6.5 31.3 %all-gather.13.cloned.1.call-start = ((), (), s32[]{:S(2)}) async-start(), calls=%async_computation.3 | async-start | bytes 1572864 | tf_op jit(solution)/shard_map/all_gather | solution.py:95
  10.8 114.0 %all-gather.15.cloned.1.call-start = ((), (), s32[]{:S(2)}) async-start(), calls=%async_computation.4 | async-start | bytes 7077888 | tf_op jit(solution)/shard_map/all_gather | solution.py:117
  11.8 212.0 %all-gather.17.cloned.1.call-start = ((), (), s32[]{:S(2)}) async-start(), calls=%async_computation.5 | async-start | bytes 7077888 | tf_op jit(solution)/shard_map/all_gather | solution.py:118
  14.4 110.4 %copy-start.15 = (f32[1536]{0:T(1024)S(1)}, f32[1536]{0:T(1024)}, u32[]{:S(2)}) copy-start(f32[1536]{0:T(1024)} %param.23) | copy-start | bytes 18436
  14.4 309.0 %all-gather.19.cloned.1.call-start = ((), (), s32[]{:S(2)}) async-start(), calls=%async_computation.6 | async-start | bytes 7077888 | tf_op jit(solution)/shard_map/all_gather | solution.py:119
  15.5 324.3 %reduce-scatter.4.cloned.1.call-start = ((), (), s32[]{:S(2)}) async-start(), calls=%async_computation.7 | async-start | bytes 1572864 | tf_op jit(solution)/shard_map/reduce_scatter | solution.py:98
  37.9 285.6 %copy-start.16 = (f32[1536]{0:T(1024)S(1)}, f32[1536]{0:T(1024)}, u32[]{:S(2)}) copy-start(f32[1536]{0:T(1024)} %param.25) | copy-start | bytes 18436
  37.9 285.6 %copy-start.13 = (bf16[256,2048]{1,0:T(8,128)(2,1)S(1)}, bf16[256,2048]{1,0:T(8,128)(2,1)}, u32[]{:S(2)}) copy-start(bf16[256,2048]{1,0:T(8,128)(2,1)} %all-gather.13.cloned.1.call-done) | copy-start | bytes 3145732
  333.1 82.8 %all-gather.25.cloned.1.call-start = ((), (), s32[]{:S(2)}) async-start(), calls=%async_computation.10 | async-start | bytes 4718592 | tf_op jit(solution)/shard_map/all_gather | solution.py:126
  334.1 91.0 %all-gather.21.cloned.1.call-start = ((), (), s32[]{:S(2)}) async-start(), calls=%async_computation.8 | async-start | bytes 1572864 | tf_op jit(solution)/shard_map/all_gather | solution.py:95
  343.4 157.8 %all-gather.27.cloned.1.call-start = ((), (), s32[]{:S(2)}) async-start(), calls=%async_computation.11 | async-start | bytes 4718592 | tf_op jit(solution)/shard_map/all_gather | solution.py:124
  344.3 23.9 %copy-start.20 = (f32[4]{0:T(128)S(1)}, f32[4]{0:T(128)}, u32[]{:S(2)}) copy-start(f32[4]{0:T(128)} %param.37) | copy-start | bytes 52
  344.3 80.7 %copy-start.17 = (f32[1024]{0:T(1024)S(1)}, f32[1024]{0:T(1024)}, u32[]{:S(2)}) copy-start(f32[1024]{0:T(1024)} %param.33) | copy-start | bytes 12292
  344.4 230.3 %all-gather.23.cloned.1.call-start = ((), (), s32[]{:S(2)}) async-start(), calls=%async_computation.9 | async-start | bytes 4718592 | tf_op jit(solution)/shard_map/all_gather | solution.py:125
  345.3 304.4 %all-gather.29.cloned.1.call-start = ((), (), s32[]{:S(2)}) async-start(), calls=%async_computation.12 | async-start | bytes 4718592 | tf_op jit(solution)/shard_map/all_gather | solution.py:131
  346.6 315.2 %reduce-scatter.6.cloned.1.call-start = ((), (), s32[]{:S(2)}) async-start(), calls=%async_computation.13 | async-start | bytes 1572864 | tf_op jit(solution)/shard_map/reduce_scatter | solution.py:98
  368.2 133.0 %copy-start.18 = (f32[1024]{0:T(1024)S(1)}, f32[1024]{0:T(1024)}, u32[]{:S(2)}) copy-start(f32[1024]{0:T(1024)} %param.29) | copy-start | bytes 12292
  430.0 144.7 %copy-start.19 = (f32[1024]{0:T(1024)S(1)}, f32[1024]{0:T(1024)}, u32[]{:S(2)}) copy-start(f32[1024]{0:T(1024)} %param.31) | copy-start | bytes 12292
  649.8 12.0 %copy-start.3 = (bf16[128,2048]{1,0:T(8,128)(2,1)S(1)}, bf16[128,2048]{1,0:T(8,128)(2,1)}, u32[]{:S(2)}) copy-start(bf16[128,2048]{1,0:T(8,128)(2,1)} %reduce-scatter.4.cloned.1.call-done) | copy-start | bytes 1572868
  655.0 20.7 %all-gather.31.cloned.1.call-start = ((), (), s32[]{:S(2)}) async-start(), calls=%async_computation.14 | async-start | bytes 1572864 | tf_op jit(solution)/shard_map/all_gather | solution.py:95
  665.4 35.9 %reduce-scatter.8.cloned.1.call-start = ((), (), s32[]{:S(2)}) async-start(), calls=%async_computation.15 | async-start | bytes 1572864 | tf_op jit(solution)/shard_map/reduce_scatter | solution.py:98
  681.9 19.3 %copy-start.4 = (bf16[128,2048]{1,0:T(8,128)(2,1)S(1)}, bf16[128,2048]{1,0:T(8,128)(2,1)}, u32[]{:S(2)}) copy-start(bf16[128,2048]{1,0:T(8,128)(2,1)} %reduce-scatter.6.cloned.1.call-done) | copy-start | bytes 1572868
  681.9 21.6 %copy-start.1 = (f32[256]{0:T(256)S(1)}, f32[256]{0:T(256)}, u32[]{:S(2)}) copy-start(f32[256]{0:T(256)} %param.36) | copy-start | bytes 3076
  (10 other events, 47.1 us)
Sparse Core Ops, SparseCore 0:
  10.9 11.7 all-gather.12
  24.9 99.8 all-gather.14
  126.9 96.8 all-gather.16
  225.8 97.6 all-gather.18
  333.2 6.5 reduce-scatter.3
  341.8 74.0 all-gather.24
  417.5 7.5 all-gather.20
  427.2 73.9 all-gather.26
  503.3 71.3 all-gather.22
  576.6 73.1 all-gather.28
  655.1 6.5 reduce-scatter.5
  665.5 10.2 all-gather.30
  691.6 9.5 reduce-scatter.7
where the time goes:
time: 711 us; the launch traced here: 710 us
  waiting for transfers between devices  551 us (77%)
  matrix products  66.8 us (9%)
  blocking collectives  43.8 us (6%)
  other arithmetic  21.5 us (3%)
  between operations  13.5 us (2%)
  local copies, waits for them, and re-layouts  12.6 us (2%)
    all_gather x1, waiting for transfers between devices, on_device(): lax.all_gather(down_b, 'fs', axis=1, tiled=True)  99.6 us
    all_gather x1, waiting for transfers between devices, on_device(): lax.all_gather(up_b, 'fs', axis=0, tiled=True)  93 us
    all_gather x1, waiting for transfers between devices, on_device(): lax.all_gather(gate_b, 'fs', axis=0, tiled=True)  86.9 us
    all_gather x1, waiting for transfers between devices, on_device(): lax.all_gather(query_b, 'fs', axis=0, tiled=True)  71.2 us
    all_gather x1, waiting for transfers between devices, on_device(): lax.all_gather(key_b, 'fs', axis=0, tiled=True)  68.6 us
    all_gather x1, waiting for transfers between devices, on_device(): lax.all_gather(value_b, 'fs', axis=0, tiled=True)  47.7 us
    all_gather x1, waiting for transfers between devices, on_device(): out_full = lax.all_gather(out_b, 'fs', axis=1, tiled=True)  42.4 us
    dot_general x3, matrix products, return_rows(): jnp.dot(hidden, weight, preferred_element_type=jnp.float32) * scale  24.4 us
  transfers between devices with their start and end apart: 13, of which 12 were waited for; matrix products, arithmetic and copies ran while one was open for 8% of the time, Pallas kernels for 0%

commit v1 on v0

--- a/solution.py
+++ b/solution.py
@@ -116,7 +116,7 @@
     held = (
         lax.all_gather(gate_b, "fs", axis=0, tiled=True),
         lax.all_gather(up_b, "fs", axis=0, tiled=True),
-        lax.all_gather(down_b, "fs", axis=1, tiled=True),
+        jnp.concatenate(lax.all_gather(down_b, "fs"), axis=1),
     )
     stream = stream + 0.5 * feed_forward(stream, norm_gains[0], held)
     gathered = gather_rows(rms_scale(stream, norm_gains[1]).astype(jnp.bfloat16))

time: 711 us -> 708 us (level)
  waiting for transfers between devices: 551 us -> 541 us
  local copies, waits for them, and re-layouts: 12.6 us -> 20.3 us
    all_gather x1, waiting for transfers between devices: 99.6 us -> 74.1 us  [on_device(): lax.all_gather(down_b, 'fs')]
    all_gather x1, waiting for transfers between devices: 86.9 us -> 102 us  [on_device(): lax.all_gather(gate_b, 'fs', axis=0, tiled=True)]
    reshape x0 -> x1, local copies, waits for them, and re-layouts: none -> 8.68 us  [on_device(): jnp.concatenate(lax.all_gather(down_b, 'fs'), axis=1)]
  transfers between devices with their start and end apart: 13 -> 13, of which waited for: 12 -> 13; matrix products, arithmetic and copies ran while one was open for 8% -> 10% of each run, Pallas kernels for 0% -> 0%
where the time goes in v1:
time: 708 us; the launch traced here: 707 us
  waiting for transfers between devices  541 us (76%)
  matrix products  66.8 us (9%)
  blocking collectives  44.4 us (6%)
  other arithmetic  20.9 us (3%)
  local copies, waits for them, and re-layouts  20.3 us (3%)
  between operations  13.6 us (2%)
    all_gather x1, waiting for transfers between devices, on_device(): lax.all_gather(gate_b, 'fs', axis=0, tiled=True)  102 us
    all_gather x1, waiting for transfers between devices, on_device(): lax.all_gather(up_b, 'fs', axis=0, tiled=True)  92.9 us
    all_gather x1, waiting for transfers between devices, on_device(): lax.all_gather(down_b, 'fs')  74.1 us
    all_gather x1, waiting for transfers between devices, on_device(): lax.all_gather(query_b, 'fs', axis=0, tiled=True)  71.2 us
    all_gather x1, waiting for transfers between devices, on_device(): lax.all_gather(key_b, 'fs', axis=0, tiled=True)  68.6 us
    all_gather x1, waiting for transfers between devices, on_device(): lax.all_gather(value_b, 'fs', axis=0, tiled=True)  47.7 us
    all_gather x1, waiting for transfers between devices, on_device(): out_full = lax.all_gather(out_b, 'fs', axis=1, tiled=True)  42.3 us
    dot_general x3, matrix products, return_rows(): jnp.dot(hidden, weight, preferred_element_type=jnp.float32) * scale  24.3 us
  transfers between devices with their start and end apart: 13, of which 13 were waited for; matrix products, arithmetic and copies ran while one was open for 10% of the time, Pallas kernels for 0%

profile of v1, /device:TPU:0, one launch (start us, length us, event | category | flops | bytes accessed | tf_op | source)
XLA Modules:
  0.0 707.3 jit_solution(12572954473191517627)
XLA Ops:
  14.0 22.9 %all-gather.1 = f32[8,1,256]{2,1,0:T(1,128)S(1)} all-gather(f32[1,1,256]{2,1,0:T(1,128)S(1)} %bitcast.121), channel_id=1, replica_groups=mesh['rep'=2,'fs'=8,'tp'=2] {'fs'}, dimensions={0}, use_global_device_ids=true | all-gather | bytes 9216 | tf_op jit(solution)/shard_map/all_gather | solution.py:83
  36.9 74.1 %all-gather.32.cloned.1.call-done = bf16[12288,256]{1,0:T(8,128)(2,1)} async-done(((bf16[1536,256]{1,0:T(8,128)(2,1)}), bf16[12288,256]{1,0:T(8,128)(2,1)}) %all-gather.32.cloned.1.call-update) | async-done | bytes 6291472 | tf_op jit(solution)/shard_map/all_gather | solution.py:119
  111.0 8.7 %copy.37 = bf16[1536,8,256]{0,2,1:T(8,128)(2,1)} copy(bf16[1536,8,256]{2,0,1:T(8,128)(2,1)} %bitcast.104) | data formatting | bytes 12582912 | tf_op jit(solution)/shard_map/reshape | solution.py:119
  119.8 102.1 %all-gather.16.cloned.1.call-done = bf16[2048,1536]{1,0:T(8,128)(2,1)} async-done(((bf16[256,1536]{1,0:T(8,128)(2,1)}), bf16[2048,1536]{1,0:T(8,128)(2,1)}) %all-gather.16.cloned.1.call-update) | async-done | bytes 6291472 | tf_op jit(solution)/shard_map/all_gather | solution.py:117
  221.9 6.1 convolution_multiply_fusion.4
  228.0 92.9 %all-gather.18.cloned.1.call-done = bf16[2048,1536]{1,0:T(8,128)(2,1)} async-done(((bf16[256,1536]{1,0:T(8,128)(2,1)}), bf16[2048,1536]{1,0:T(8,128)(2,1)}) %all-gather.18.cloned.1.call-update) | async-done | bytes 6291472 | tf_op jit(solution)/shard_map/all_gather | solution.py:118
  320.9 9.6 %fusion.46 = bf16[256,2048]{1,0:T(8,128)(2,1)} fusion(bf16[1536,2048]{0,1:T(8,128)(2,1)} %bitcast.102, f32[2048]{0:T(1024)S(1)} %bitcast.119, bf16[256,2048]{1,0:T(8,128)(2,1)S(1)} %copy-done.13, bf16[2048,1536]{1,0:T(8,128)(2,1)} %all-gather.18.cloned.1.call-done, f32[256,1536]{1,0:T(8,128)} %convolution_multiply_fusion.4, f32[1536]{0:T(1024)S(1)} %copy-done.16), kind=kOutput, calls=%fused_computation.50 | convolution fusion | flops 3225026560 | bytes 16267264 | tf_op jit(solution)/shard_map/dot_general | solution.py:99
  331.5 5.7 reduce-scatter.4.cloned.1.call-done
  344.0 21.5 %all-gather.2 = f32[8,1,256]{2,1,0:T(1,128)S(1)} all-gather(f32[1,1,256]{2,1,0:T(1,128)S(1)} %bitcast.122), channel_id=1, replica_groups=mesh['rep'=2,'fs'=8,'tp'=2] {'fs'}, dimensions={0}, use_global_device_ids=true | all-gather | bytes 9216 | tf_op jit(solution)/shard_map/all_gather | solution.py:84
  365.6 47.7 %all-gather.24.cloned.1.call-done = bf16[2048,1024]{1,0:T(8,128)(2,1)} async-done(((bf16[256,1024]{1,0:T(8,128)(2,1)}), bf16[2048,1024]{1,0:T(8,128)(2,1)}) %all-gather.24.cloned.1.call-update) | async-done | bytes 4194320 | tf_op jit(solution)/shard_map/all_gather | solution.py:126
  413.3 9.1 %all-gather.20.cloned.1.call-done = bf16[256,2048]{1,0:T(8,128)(2,1)} async-done(((bf16[128,2048]{1,0:T(8,128)(2,1)}), bf16[256,2048]{1,0:T(8,128)(2,1)}) %all-gather.20.cloned.1.call-update) | async-done | bytes 1048592 | tf_op jit(solution)/shard_map/all_gather | solution.py:95
  422.5 3.8 fusion.53
  427.4 71.2 %all-gather.26.cloned.1.call-done = bf16[2048,1024]{1,0:T(8,128)(2,1)} async-done(((bf16[256,1024]{1,0:T(8,128)(2,1)}), bf16[2048,1024]{1,0:T(8,128)(2,1)}) %all-gather.26.cloned.1.call-update) | async-done | bytes 4194320 | tf_op jit(solution)/shard_map/all_gather | solution.py:124
  498.6 3.8 fusion.54
  503.5 68.6 %all-gather.22.cloned.1.call-done = bf16[2048,1024]{1,0:T(8,128)(2,1)} async-done(((bf16[256,1024]{1,0:T(8,128)(2,1)}), bf16[2048,1024]{1,0:T(8,128)(2,1)}) %all-gather.22.cloned.1.call-update) | async-done | bytes 4194320 | tf_op jit(solution)/shard_map/all_gather | solution.py:125
  572.1 3.8 fusion.52
  580.5 19.3 %while.15 = (s32[]{:T(128)}, f32[4,256,256]{2,1,0:T(8,128)S(1)}, f32[4,4,64,256]{3,2,1,0:T(8,128)S(1)}, f32[4,1,1]{0,2,1:T(1,128)S(1)}, bf16[4,4,64,256]{3,2,1,0...) while((s32[]{:T(128)}, f32[4,256,256]{2,1,0:T(8,128)S(1)}, ...), condition=%wide.region_4.5_spmd.clone.clone.clone, body=%wide.region_3.4_spmd.clone.clone.clone.sunk | while | flops 420856320 | bytes 4761488 | solution.py:51
  604.8 42.3 %all-gather.28.cloned.1.call-done = bf16[1024,2048]{1,0:T(8,128)(2,1)} async-done(((bf16[1024,256]{1,0:T(8,128)(2,1)}), bf16[1024,2048]{1,0:T(8,128)(2,1)}) %all-gather.28.cloned.1.call-update) | async-done | bytes 4194320 | tf_op jit(solution)/shard_map/all_gather | solution.py:131
  647.2 5.2 fusion.48
  652.4 6.7 reduce-scatter.6.cloned.1.call-done
  663.0 10.1 %all-gather.30.cloned.1.call-done = bf16[256,2048]{1,0:T(8,128)(2,1)} async-done(((bf16[128,2048]{1,0:T(8,128)(2,1)}), bf16[256,2048]{1,0:T(8,128)(2,1)}) %all-gather.30.cloned.1.call-update) | async-done | bytes 1048592 | tf_op jit(solution)/shard_map/all_gather | solution.py:95
  673.1 6.1 convolution_multiply_fusion.2
  679.3 9.6 %fusion.47 = bf16[256,2048]{1,0:T(8,128)(2,1)} fusion(bf16[1536,2048]{0,1:T(8,128)(2,1)} %bitcast.103, f32[2048]{0:T(1024)S(1)} %bitcast.120, bf16[256,2048]{1,0:T(8,128)(2,1)S(1)} %copy-done.14, bf16[2048,1536]{1,0:T(8,128)(2,1)} %all-gather.18.cloned.1.call-done, f32[256,1536]{1,0:T(8,128)} %convolution_multiply_fusion.2, f32[1536]{0:T(1024)S(1)} %copy-done.16), kind=kOutput, calls=%fused_computation.51 | convolution fusion | flops 3225026560 | bytes 16267264 | tf_op jit(solution)/shard_map/dot_general | solution.py:99
  688.8 9.7 %reduce-scatter.8.cloned.1.call-done = bf16[128,2048]{1,0:T(8,128)(2,1)} async-done(((bf16[256,2048]{1,0:T(8,128)(2,1)}), bf16[128,2048]{1,0:T(8,128)(2,1)}) %reduce-scatter.8.cloned.1.call-update) | async-done | bytes 524304 | tf_op jit(solution)/shard_map/reduce_scatter | solution.py:98
  (127 shorter events, 52.6 us)
Async XLA Ops:
  6.5 337.5 %copy-start = (f32[256]{0:T(256)S(1)}, f32[256]{0:T(256)}, u32[]{:S(2)}) copy-start(f32[256]{0:T(256)} %param.36) | copy-start | bytes 3076
  6.5 104.5 %all-gather.32.cloned.1.call-start = ((), (), s32[]{:S(2)}) async-start(), calls=%async_computation.15 | async-start | bytes 7077888 | tf_op jit(solution)/shard_map/all_gather | solution.py:119
  9.1 110.7 %all-gather.14.cloned.1.call-start = ((), (), s32[]{:S(2)}) async-start(), calls=%async_computation.3 | async-start | bytes 1572864 | tf_op jit(solution)/shard_map/all_gather | solution.py:95
  10.4 211.5 %all-gather.16.cloned.1.call-start = ((), (), s32[]{:S(2)}) async-start(), calls=%async_computation.4 | async-start | bytes 7077888 | tf_op jit(solution)/shard_map/all_gather | solution.py:117
  11.5 309.4 %all-gather.18.cloned.1.call-start = ((), (), s32[]{:S(2)}) async-start(), calls=%async_computation.5 | async-start | bytes 7077888 | tf_op jit(solution)/shard_map/all_gather | solution.py:118
  14.0 323.2 %reduce-scatter.4.cloned.1.call-start = ((), (), s32[]{:S(2)}) async-start(), calls=%async_computation.6 | async-start | bytes 1572864 | tf_op jit(solution)/shard_map/reduce_scatter | solution.py:98
  111.0 110.9 %copy-start.15 = (f32[1536]{0:T(1024)S(1)}, f32[1536]{0:T(1024)}, u32[]{:S(2)}) copy-start(f32[1536]{0:T(1024)} %param.23) | copy-start | bytes 18436
  119.7 201.1 %copy-start.16 = (f32[1536]{0:T(1024)S(1)}, f32[1536]{0:T(1024)}, u32[]{:S(2)}) copy-start(f32[1536]{0:T(1024)} %param.25) | copy-start | bytes 18436
  119.8 201.0 %copy-start.13 = (bf16[256,2048]{1,0:T(8,128)(2,1)S(1)}, bf16[256,2048]{1,0:T(8,128)(2,1)}, u32[]{:S(2)}) copy-start(bf16[256,2048]{1,0:T(8,128)(2,1)} %all-gather.14.cloned.1.call-done) | copy-start | bytes 3145732
  330.5 82.8 %all-gather.24.cloned.1.call-start = ((), (), s32[]{:S(2)}) async-start(), calls=%async_computation.9 | async-start | bytes 4718592 | tf_op jit(solution)/shard_map/all_gather | solution.py:126
  331.5 91.0 %all-gather.20.cloned.1.call-start = ((), (), s32[]{:S(2)}) async-start(), calls=%async_computation.7 | async-start | bytes 1572864 | tf_op jit(solution)/shard_map/all_gather | solution.py:95
  340.7 157.8 %all-gather.26.cloned.1.call-start = ((), (), s32[]{:S(2)}) async-start(), calls=%async_computation.10 | async-start | bytes 4718592 | tf_op jit(solution)/shard_map/all_gather | solution.py:124
  341.7 23.9 %copy-start.20 = (f32[4]{0:T(128)S(1)}, f32[4]{0:T(128)}, u32[]{:S(2)}) copy-start(f32[4]{0:T(128)} %param.37) | copy-start | bytes 52
  341.7 80.7 %copy-start.17 = (f32[1024]{0:T(1024)S(1)}, f32[1024]{0:T(1024)}, u32[]{:S(2)}) copy-start(f32[1024]{0:T(1024)} %param.33) | copy-start | bytes 12292
  341.7 230.3 %all-gather.22.cloned.1.call-start = ((), (), s32[]{:S(2)}) async-start(), calls=%async_computation.8 | async-start | bytes 4718592 | tf_op jit(solution)/shard_map/all_gather | solution.py:125
  342.7 304.5 %all-gather.28.cloned.1.call-start = ((), (), s32[]{:S(2)}) async-start(), calls=%async_computation.11 | async-start | bytes 4718592 | tf_op jit(solution)/shard_map/all_gather | solution.py:131
  343.9 315.2 %reduce-scatter.6.cloned.1.call-start = ((), (), s32[]{:S(2)}) async-start(), calls=%async_computation.12 | async-start | bytes 1572864 | tf_op jit(solution)/shard_map/reduce_scatter | solution.py:98
  365.6 133.0 %copy-start.18 = (f32[1024]{0:T(1024)S(1)}, f32[1024]{0:T(1024)}, u32[]{:S(2)}) copy-start(f32[1024]{0:T(1024)} %param.29) | copy-start | bytes 12292
  427.4 144.7 %copy-start.19 = (f32[1024]{0:T(1024)S(1)}, f32[1024]{0:T(1024)}, u32[]{:S(2)}) copy-start(f32[1024]{0:T(1024)} %param.31) | copy-start | bytes 12292
  647.2 12.0 %copy-start.3 = (bf16[128,2048]{1,0:T(8,128)(2,1)S(1)}, bf16[128,2048]{1,0:T(8,128)(2,1)}, u32[]{:S(2)}) copy-start(bf16[128,2048]{1,0:T(8,128)(2,1)} %reduce-scatter.4.cloned.1.call-done) | copy-start | bytes 1572868
  652.4 20.8 %all-gather.30.cloned.1.call-start = ((), (), s32[]{:S(2)}) async-start(), calls=%async_computation.13 | async-start | bytes 1572864 | tf_op jit(solution)/shard_map/all_gather | solution.py:95
  662.7 35.8 %reduce-scatter.8.cloned.1.call-start = ((), (), s32[]{:S(2)}) async-start(), calls=%async_computation.14 | async-start | bytes 1572864 | tf_op jit(solution)/shard_map/reduce_scatter | solution.py:98
  679.3 19.3 %copy-start.4 = (bf16[128,2048]{1,0:T(8,128)(2,1)S(1)}, bf16[128,2048]{1,0:T(8,128)(2,1)}, u32[]{:S(2)}) copy-start(bf16[128,2048]{1,0:T(8,128)(2,1)} %reduce-scatter.6.cloned.1.call-done) | copy-start | bytes 1572868
  679.3 21.5 %copy-start.1 = (f32[256]{0:T(256)S(1)}, f32[256]{0:T(256)}, u32[]{:S(2)}) copy-start(f32[256]{0:T(256)} %param.36) | copy-start | bytes 3076
  (10 other events, 44.2 us)
Sparse Core Ops, SparseCore 0:
  9.5 101.4 all-gather.31
  112.6 7.1 all-gather.13
  122.0 99.8 all-gather.15
  224.0 96.8 all-gather.17
  330.6 6.5 reduce-scatter.3
  339.2 74.1 all-gather.23
  414.9 7.5 all-gather.19
  424.6 73.9 all-gather.25
  500.7 71.3 all-gather.21
  574.0 73.1 all-gather.27
  652.5 6.5 reduce-scatter.5
  662.9 10.2 all-gather.29
  689.0 9.5 reduce-scatter.7
